TPU v7x, 32 devices: a whole 2x2x4 slice. The times are simulated.
32 devices in a mesh: ep: 8 (over z, core), tp: 4 (over y, x).
Axes of the slice: x: 2, y: 2, z: 4, core: 2. Of those that a mesh axis runs over, the one named last changes fastest.
Arguments:
- tokens: bfloat16 [1024, 2048], P('ep', 'tp')
- norm_gain: float32 [2048], P('tp'), may hold values from 0.1 to 1.9
- routing: int32 [1024, 2], P('ep'), may hold values from 0 to 3, all different within a row; in each aligned block of 128 rows (0 to 127, 128 to 255, ...) at most 80 rows name the same one
- route_weight: float32 [1024, 2], P('ep'), may hold values from 0.1 to 1
- gate_weight: bfloat16 [8, 2048, 3584], P('ep', None, 'tp'), may hold values from -0.125 to 0.125
- up_weight: bfloat16 [8, 2048, 3584], P('ep', None, 'tp'), may hold values from -0.125 to 0.125
- down_weight: bfloat16 [8, 3584, 2048], P('ep', None, 'tp')
- final_gain: float32 [2048], P('tp'), may hold values from 0.1 to 1.9
Outputs:
- mixed: bfloat16 [1024, 2048], P('ep', 'tp')
Inputs may be any that keep to these rules, and one draw needn't show every extreme that they name: `routing`: each row names 2 different experts. Among the 128 rows of one device along ep (aligned blocks), no expert is named more than 80 times, a bound that some blocks reach.
All inputs are finite; a program needn't handle non-finite values.
Results may differ from a plain program's by a relative error of at most 0.0077.
Values may be sent and summed in bfloat16 or wider, within the bound.
A program may use at most 64 MiB of HBM per device.

v0:
```python
import jax
import jax.numpy as jnp
from jax import lax
from jax.sharding import PartitionSpec as P

D = 2048
TOPK = 2


EPS = 1e-05


def from_partner(shard, axis, apart):
    return lax.ppermute(shard, axis, [(i, i ^ 1 << apart) for i in range(lax.axis_size(axis))])


def shards(
    tokens, norm_gain, routing, route_weight, gate_weight, up_weight, down_weight, final_gain
):
    ep_count = lax.axis_size("ep")
    experts = ep_count // 2
    tok_rows = tokens.shape[0]
    width_local = tokens.shape[1]
    capacity = 2 * ((tok_rows * TOPK * 5 + experts * 8 - 1) // (experts * 8))
    half_cap = capacity // 2
    row_count = ep_count * capacity
    is_even = lax.axis_index("ep") % 2 == 0
    values_f = tokens.astype(jnp.float32)
    square_sum = lax.psum(jnp.sum(values_f * values_f, axis=1), "tp")
    normed = (values_f * lax.rsqrt(square_sum / D + EPS)[:, None] * norm_gain).astype(jnp.bfloat16)
    expert_ids = routing.reshape(-1)
    onehot = (expert_ids[:, None] == jnp.arange(experts, dtype=jnp.int32)).astype(jnp.int32)
    slot_index = jnp.sum((jnp.cumsum(onehot, axis=0) - onehot) * onehot, axis=1)
    place_index = expert_ids * capacity + slot_index
    hit_table = (place_index[:, None] == jnp.arange(experts * capacity, dtype=jnp.int32)).astype(
        jnp.float32
    )
    hit_table = hit_table.reshape(tok_rows, TOPK, experts * capacity)
    picker = jnp.sum(hit_table, axis=1)
    weighted = jnp.sum(hit_table * route_weight[:, :, None], axis=1)
    contract = (((0,), (0,)), ((), ()))
    gate_local = gate_weight[0]
    up_local = up_weight[0]
    down_local = down_weight[0]
    picker_pair = jnp.broadcast_to(
        picker.reshape(tok_rows, experts, 1, capacity), (tok_rows, experts, 2, capacity)
    )
    picker_pair = picker_pair.reshape(tok_rows, row_count).astype(jnp.bfloat16)
    outgoing = lax.dot_general(picker_pair, normed, contract, preferred_element_type=jnp.float32)
    outgoing = outgoing.astype(jnp.bfloat16).reshape(ep_count, capacity, width_local)
    arrived = lax.all_to_all(outgoing, "ep", split_axis=0, concat_axis=0, tiled=True).reshape(
        row_count, width_local
    )
    shard_piece = lax.all_gather(arrived, "tp", axis=1, tiled=True)
    gate = jnp.dot(shard_piece, gate_local, preferred_element_type=jnp.float32)
    upper = jnp.dot(shard_piece, up_local, preferred_element_type=jnp.float32)
    hidden = (jax.nn.silu(gate) * upper).astype(jnp.bfloat16)
    half_out = jnp.dot(
        lax.all_gather(hidden, "tp", axis=1, tiled=True),
        down_local,
        preferred_element_type=jnp.float32,
    )
    half_out = half_out.astype(jnp.bfloat16).reshape(ep_count, capacity, width_local)
    partner_out = from_partner(half_out, "ep", 0)
    pair_sum = (half_out.astype(jnp.float32) + partner_out.astype(jnp.float32)).astype(jnp.bfloat16)
    start = jnp.where(is_even, 0, half_cap).astype(jnp.int32)
    own_slots = lax.dynamic_slice_in_dim(pair_sum, start, half_cap, 1)
    paired = lax.all_to_all(own_slots, "ep", split_axis=0, concat_axis=0, tiled=True)
    paired = lax.optimization_barrier(paired)
    paired = paired.reshape(experts * capacity, width_local).astype(jnp.float32)
    mixed_sum = jnp.dot(weighted, paired, precision=lax.Precision.HIGHEST)
    out_square = lax.psum(jnp.sum(mixed_sum * mixed_sum, axis=1), "tp")
    return (mixed_sum * lax.rsqrt(out_square / D + EPS)[:, None] * final_gain).astype(jnp.bfloat16)


def solution(mesh):
    placed = (
        P("ep", "tp"),
        P("tp"),
        P("ep", None),
        P("ep", None),
        P("ep", None, "tp"),
        P("ep", None, "tp"),
        P("ep", None, "tp"),
        P("tp"),
    )
    return jax.shard_map(
        shards, mesh=mesh, in_specs=placed, out_specs=P("ep", "tp"), check_vma=False
    )
```

profile of v0, /device:TPU:0, one launch (start us, length us, event | category | flops | bytes accessed | tf_op | source)
XLA Modules:
  0.0 190.9 jit_solution(4550123394074367426)
XLA Ops:
  6.5 0.8 copy.27
  7.3 0.1 eq.48
  7.5 0.1 eq.44
  7.6 1.2 reduce-window.6
  8.8 0.1 slice.8
  8.9 0.1 copy.29
  9.1 0.1 copy.30
  9.2 0.1 add_bitcast_fusion
  9.3 0.1 reduce_sum.48
  9.4 0.1 copy.31
  9.5 0.7 multiply_add_fusion
  10.2 1.0 fusion.11
  11.2 11.4 %psum.14 = f32[128]{0:T(128)S(1)} all-reduce(f32[128]{0:T(128)S(1)} %fusion.11), channel_id=1, replica_groups=mesh['ep'=8,'tp'=4] {'tp'}, use_global_device_ids=true, to_apply=%region_6.7 | all-reduce | flops 128 | bytes 1024 | tf_op jit(solution)/shard_map/psum | solution.py:29
  22.6 0.8 convert_reduce_fusion
  23.4 1.3 convolution_convert_fusion
  24.7 22.9 %all_to_all.10 = bf16[8,80,512]{2,1,0:T(8,128)(2,1)} all-to-all(bf16[8,80,512]{2,1,0:T(8,128)(2,1)S(1)} %bitcast.45), channel_id=1, replica_groups=mesh['ep'=8,'tp'=4] {'ep'}, dimensions={0} | all-to-all | bytes 1310720 | tf_op jit(solution)/shard_map/all_to_all | solution.py:51
  47.6 0.0 all-gather.3.cloned.1.call-update
  47.6 0.0 all-gather.5.cloned.1.call-start
  47.7 36.5 %all-gather.3.cloned.1.call-done = bf16[640,2048]{1,0:T(8,128)(2,1)} async-done(((bf16[640,512]{1,0:T(8,128)(2,1)}), bf16[640,2048]{1,0:T(8,128)(2,1)}) %all-gather.3.cloned.1.call-update) | async-done | bytes 2621456 | tf_op jit(solution)/shard_map/all_gather | solution.py:54
  84.2 5.8 %fusion.4 = f32[640,896]{1,0:T(8,128)S(1)} fusion(bf16[640,2048]{1,0:T(8,128)(2,1)} %all-gather.3.cloned.1.call-done, bf16[1,2048,896]{2,1,0:T(8,128)(2,1)} %param.12), kind=kOutput, calls=%fused_computation.4 | convolution fusion | flops 2348810240 | bytes 8585216 | tf_op jit(solution)/shard_map/dot_general | solution.py:55
  90.1 4.0 %multiply_convert_fusion = bf16[640,896]{1,0:T(8,128)(2,1)} fusion(f32[640,896]{1,0:T(8,128)S(1)} %fusion.4, bf16[640,2048]{1,0:T(8,128)(2,1)S(1)} %copy-done.2, bf16[1,2048,896]{2,1,0:T(8,128)(2,1)S(1)} %copy-done.1), kind=kOutput, calls=%fused_computation.6 | convolution fusion | flops 2352250880 | bytes 9732096 | tf_op jit(solution)/shard_map/dot_general | solution.py:56
  94.1 0.0 all-gather.5.cloned.1.call-update
  94.1 0.0 copy-start
  94.1 56.0 %all-gather.5.cloned.1.call-done = bf16[640,3584]{1,0:T(8,128)(2,1)} async-done(((bf16[640,896]{1,0:T(8,128)(2,1)}), bf16[640,3584]{1,0:T(8,128)(2,1)}) %all-gather.5.cloned.1.call-update) | async-done | bytes 4587536 | tf_op jit(solution)/shard_map/all_gather | solution.py:59
  150.1 6.0 %fusion.8 = bf16[640,512]{1,0:T(8,128)(2,1)S(1)} fusion(bf16[640,3584]{1,0:T(8,128)(2,1)} %all-gather.5.cloned.1.call-done, bf16[1,3584,512]{2,1,0:T(8,128)(2,1)} %param.14), kind=kOutput, calls=%fused_computation.8 | convolution fusion | flops 2349137920 | bytes 8912896 | tf_op jit(solution)/shard_map/dot_general | solution.py:58
  156.1 0.1 collective-permute-start
  156.2 2.1 %collective-permute-done = bf16[8,80,512]{2,1,0:T(8,128)(2,1)S(1)} collective-permute-done((bf16[8,80,512]{2,1,0:T(8,128)(2,1)S(1)}, bf16[8,80,512]{2,1,0:T(8,128)(2,1)S(1)}, u32[]{:S(2)}, u32[]{:S(2)}) %collective-permute-start) | collective-permute-done | bytes 655392 | tf_op jit(solution)/shard_map/ppermute | solution.py:14
  158.3 0.1 add_convert_fusion
  158.4 15.5 %all_to_all.11 = bf16[8,40,512]{2,1,0:T(8,128)(2,1)S(1)} all-to-all(bf16[8,40,512]{2,1,0:T(8,128)(2,1)S(1)} %add_convert_fusion), channel_id=1, replica_groups=mesh['ep'=8,'tp'=4] {'ep'}, dimensions={0} | all-to-all | bytes 655360 | tf_op jit(solution)/shard_map/all_to_all | solution.py:68
  173.9 0.5 multiply_reduce_fusion
  174.4 8.9 %psum.15 = f32[128]{0:T(128)S(1)} all-reduce(f32[128]{0:T(128)S(1)} %get-tuple-element.7), channel_id=1, replica_groups=mesh['ep'=8,'tp'=4] {'tp'}, use_global_device_ids=true, to_apply=%region_8.9 | all-reduce | flops 128 | bytes 1024 | tf_op jit(solution)/shard_map/psum | solution.py:72
  183.3 0.8 multiply_convert_fusion.1
  (13 shorter events, 0.1 us)
Async XLA Ops:
  6.5 77.7 %all-gather.3.cloned.1.call-start = ((), (), s32[]{:S(2)}) async-start(), calls=%async_computation.2 | async-start | bytes 3276800 | tf_op jit(solution)/shard_map/all_gather | solution.py:54
  47.6 102.5 %all-gather.5.cloned.1.call-start = ((), (), s32[]{:S(2)}) async-start(), calls=%async_computation.3 | async-start | bytes 5734400 | tf_op jit(solution)/shard_map/all_gather | solution.py:59
  84.2 5.8 %copy-start.1 = (bf16[1,2048,896]{2,1,0:T(8,128)(2,1)S(1)}, bf16[1,2048,896]{2,1,0:T(8,128)(2,1)}, u32[]{:S(2)}) copy-start(bf16[1,2048,896]{2,1,0:T(8,128)(2,1)} %param.13) | copy-start | bytes 11010052
  84.2 5.9 %copy-start.2 = (bf16[640,2048]{1,0:T(8,128)(2,1)S(1)}, bf16[640,2048]{1,0:T(8,128)(2,1)}, u32[]{:S(2)}) copy-start(bf16[640,2048]{1,0:T(8,128)(2,1)} %all-gather.3.cloned.1.call-done) | copy-start | bytes 7864324
  94.1 89.2 %copy-start = (f32[512]{0:T(512)S(1)}, f32[512]{0:T(512)}, u32[]{:S(2)}) copy-start(f32[512]{0:T(512)} %param.15) | copy-start | bytes 6148
  156.1 2.2 %collective-permute-start = (bf16[8,80,512]{2,1,0:T(8,128)(2,1)S(1)}, bf16[8,80,512]{2,1,0:T(8,128)(2,1)S(1)}, u32[]{:S(2)}, u32[]{:S(2)}) collective-permute-start(bf16[8,80,512]{2,1,0:T(8,128)(2,1)S(1)} %bitcast.49), channel_id=1, source_target_pairs={{0,4},{4,0},{8,12},{12,8},{16,20},{20,16},{24,28},{28,24},{1,5},{5... | collective-permute-start | bytes 1966088 | tf_op jit(solution)/shard_map/ppermute | solution.py:14
Sparse Core Ops, SparseCore 0:
  47.8 36.4 all-gather.2
  94.3 55.8 all-gather.4
where the time goes:
time: 191 us
  waiting for transfers between devices  94.6 us (50%)
  blocking collectives  58.8 us (31%)
  matrix products  17.6 us (9%)
  between operations  13.5 us (7%)
  other arithmetic  4.71 us (2%)
    all_gather x1, waiting for transfers between devices, shards(): lax.all_gather(hidden, 'tp', axis=1, tiled=True)  56 us
    all_gather x1, waiting for transfers between devices, shards(): shard_piece = lax.all_gather(arrived, 'tp', axis=1, tiled=True)  36.5 us
    all_to_all x1, blocking collectives, shards(): lax.all_to_all(outgoing, 'ep', split_axis=0, concat_axis=0, tiled=True)  22.9 us
    all_to_all x1, blocking collectives, shards(): lax.all_to_all(own_slots, 'ep', split_axis=0, concat_axis=0, tiled=True)  15.5 us
    psum x1, blocking collectives, shards(): square_sum = lax.psum(jnp.sum(values_f * values_f, axis=1), 'tp')  11.4 us
    psum x1, blocking collectives, shards(): out_square = lax.psum(jnp.sum(mixed_sum * mixed_sum, axis=1), 'tp')  8.93 us
    dot_general x1, matrix products, shards(): jnp.dot(lax.all_gather(hidden, 'tp', axis=1, tiled=True), down_local, pre...  5.96 us
    dot_general x1, matrix products, shards(): gate = jnp.dot(shard_piece, gate_local, preferred_element_type=jnp.float32)  5.84 us
  transfers between devices with their start and end apart: 3, of which 3 were waited for; matrix products, arithmetic and copies ran while one was open for 0% of the time, Pallas kernels for 0%

commit v1 on v0

v1 whole, which is shorter than its diff:
```python
import functools

import jax
import jax.numpy as jnp
from jax import lax
from jax.experimental import pallas as pl
from jax.experimental.pallas import tpu as pltpu
from jax.sharding import PartitionSpec as P

TOPK = 2
EPS = 1e-05
MESH = pl.DeviceIdType.MESH
F32, BF16 = jnp.float32, jnp.bfloat16


def flipped(index, mask):
    out, bit = index, 1
    while bit <= mask:
        if mask & bit:
            out = out + bit - 2 * bit * ((index // bit) % 2)
        bit *= 2
    return out


def dot(a, b):
    return jnp.dot(a, b, preferred_element_type=F32)


def kernel(
    n, planes, groups,
    tokens, gain, routing, routing_t, route_weight, gate_hbm, up_hbm, down_hbm, final_gain,
    out,
    wg, wu, wd, gains, picked, x, xn, hid, half_own, half_send, half_recv, pair, comb, sq_out, sq_in,
    w_sem, gain_s, gain_r, disp_s, disp_r, x_s, x_r, d2d_s, d2d_r, h_s, h_r, po_s, po_r, c_s, c_r,
    sq_s, sq_r,
):
    ep, t = lax.axis_index("ep"), lax.axis_index("tp")
    z, core = ep // 2, ep % 2
    partner = (ep + 1 - 2 * core, t)
    cap, width = picked.shape[1], picked.shape[2]
    per = planes // groups
    rows = per * cap
    inner = hid.shape[-1]
    tok_rows = tokens.shape[0]
    depth = n * width
    bits = [1 << b for b in range(n.bit_length() - 1)]
    tp_peer = [(ep, flipped(t, j)) for j in range(n)]
    tp_index = [flipped(t, j) for j in range(n)]
    expert = [flipped(z, k) for k in range(planes)]
    plane_peer = [(2 * expert[k] + core, t) for k in range(planes)]

    loads = [
        pltpu.make_async_copy(src.at[0], dst, w_sem.at[i])
        for i, (src, dst) in enumerate(((gate_hbm, wg), (up_hbm, wu), (down_hbm, wd)))
    ]
    for load in loads:
        load.start()

    barrier = pltpu.get_barrier_semaphore()
    peers = tp_peer[1:] + plane_peer[1:] + [partner]
    for peer in peers:
        pl.semaphore_signal(barrier, inc=1, device_id=peer, device_id_type=MESH)

    token_row = lax.broadcasted_iota(jnp.int32, (tok_rows, tok_rows), 0)
    token_col = lax.broadcasted_iota(jnp.int32, (tok_rows, tok_rows), 1)
    r_t0, r_t1 = routing_t[0:1, :], routing_t[1:2, :]
    wide = -(-planes // 16) * 16
    sub = lax.broadcasted_iota(jnp.int32, (wide, tok_rows), 0)
    member_t = jnp.zeros((wide, tok_rows), F32)
    for k in range(planes):
        named = ((r_t0 == expert[k]) | (r_t1 == expert[k])).astype(F32)
        member_t = jnp.where(sub == k, named, member_t)
    earlier = (token_row < token_col).astype(F32).astype(BF16)
    slot_t = dot(member_t.astype(BF16), earlier)
    slot_t = jnp.where(member_t > 0, slot_t, -1.0)
    slot_sub = lax.broadcasted_iota(jnp.int32, (cap, tok_rows), 0).astype(F32)

    def pick(k):
        chosen = (slot_sub == slot_t[k : k + 1, :]).astype(F32).astype(BF16)
        return dot(chosen, tokens[...]).astype(BF16)

    sent = []

    def remote(src, dst, s, r, peer):
        return pltpu.make_async_remote_copy(
            src_ref=src, dst_ref=dst, send_sem=s, recv_sem=r, device_id=peer, device_id_type=MESH
        )

    def start(copy):
        copy.start()
        sent.append(copy)
        return copy

    for k in range(1, planes):
        picked[k] = pick(k)
    x[0, 0, 0, 0] = pick(0)

    pl.semaphore_wait(barrier, len(peers))

    disp = [
        None if k == 0 else remote(
            picked.at[k], x.at[k // per, 0, 0, k % per], disp_s.at[k], disp_r.at[k], plane_peer[k]
        )
        for k in range(planes)
    ]
    for k in range(1, planes):
        start(disp[k])

    def tree(at, send_sem, recv_sem, order):
        copies, need = {}, {0: []}
        have = [0]
        for position, bit in enumerate(order):
            for j in list(have):
                into = j ^ bit
                copies[into] = remote(at(j), at(into), send_sem(into), recv_sem(into), tp_peer[bit])
                need[j].append(into)
                need[into] = []
                have.append(into)
        return copies, need, have[1:]

    def ascending(g):
        return bits if g % 2 == 0 else bits[::-1]

    trees = [
        tree(
            lambda j, g=g: x.at[g, j, 0], lambda j, g=g: x_s.at[g, j],
            lambda j, g=g: x_r.at[g, j], ascending(g),
        )
        for g in range(groups)
    ]
    across = [
        [remote(x.at[g, j, 0], x.at[g, j, 1], d2d_s.at[g, j], d2d_r.at[g, j], partner) for j in range(n)]
        for g in range(groups)
    ]
    hidden_trees = [
        [
            tree(
                lambda j, g=g, side=side: hid.at[g, j, side],
                lambda j, g=g, side=side: h_s.at[g, side, j],
                lambda j, g=g, side=side: h_r.at[g, side, j], ascending(side),
            )
            for side in range(2)
        ]
        for g in range(groups)
    ]

    def gather_start(g):
        for k in range(max(1, g * per), (g + 1) * per):
            disp[k].wait_recv()
        copies, need, _ = trees[g]
        for into in need[0]:
            start(copies[into])
        start(across[g][0])

    def gather_relay(g):
        copies, need, arrivals = trees[g]
        for j in arrivals:
            if need[j]:
                copies[j].wait_recv()
                for into in need[j]:
                    start(copies[into])
                start(across[g][j])

    def gather_end(g):
        copies, need, arrivals = trees[g]
        for j in arrivals:
            if not need[j]:
                copies[j].wait_recv()
                start(across[g][j])
        for j in range(n):
            across[g][j].wait_recv()

    def upward(g):
        parts = [x[g, j].reshape(2 * rows, width).astype(F32) for j in range(n)]
        square = sum(jnp.sum(p * p, axis=1, keepdims=True) for p in parts)
        scale = lax.rsqrt(square / depth + EPS)
        for j in range(n):
            columns = pl.ds(pl.multiple_of(tp_index[j] * width, width), width)
            xn[:, columns] = (parts[j] * scale * gains[j]).astype(BF16)
        for first in range(0, inner, 256):
            last = min(first + 256, inner)
            left = dot(xn[...], wg[:, first:last])
            right = dot(xn[...], wu[:, first:last])
            value = (jax.nn.silu(left) * right).astype(BF16)
            hid[g, 0, :, :, first:last] = value.reshape(2, rows, last - first)
        for step in range(len(bits)):
            for side in range(2):
                copies, need, _ = hidden_trees[g][side]
                start(copies[need[0][step]])

    def hidden_relay(g):
        for side in range(2):
            copies, need, arrivals = hidden_trees[g][side]
            for j in arrivals:
                if need[j]:
                    copies[j].wait_recv()
                    for into in need[j]:
                        start(copies[into])

    halves = [
        remote(half_send.at[g], half_recv.at[g], po_s.at[g], po_r.at[g], partner) for g in range(groups)
    ]

    def downward(g):
        for side in range(2):
            copies, need, arrivals = hidden_trees[g][side]
            for j in arrivals:
                if not need[j]:
                    copies[j].wait_recv()
        total = None
        for j in range(n):
            part = wd[pl.ds(pl.multiple_of(tp_index[j] * inner, inner), inner), :]
            term = dot(hid[g, j].reshape(2 * rows, inner), part)
            total = term if total is None else total + term
        half_own[g] = total[:rows].astype(BF16)
        half_send[g] = total[rows:].astype(BF16)
        start(halves[g])

    back = [
        None if k == 0 else remote(
            pair.at[k // per, k % per], comb.at[k], c_s.at[k], c_r.at[k], plane_peer[k]
        )
        for k in range(planes)
    ]

    def combine(g):
        halves[g].wait_recv()
        both = (half_own[g].astype(F32) + half_recv[g].astype(F32)).astype(BF16)
        pair[g] = both.reshape(per, cap, width)
        for k in range(g * per, (g + 1) * per):
            if k == 0:
                comb[0] = both[:cap]
            else:
                start(back[k])

    gather_start(0)
    gain_copies = [
        remote(gain, gains.at[j], gain_s.at[j], gain_r.at[j], tp_peer[j]) for j in range(1, n)
    ]
    for copy in gain_copies:
        start(copy)
    gains[0] = gain[...]
    if groups > 1:
        gather_start(1)
    gather_relay(0)
    for copy in gain_copies:
        copy.wait_recv()
    loads[0].wait()
    loads[1].wait()
    for g in range(groups):
        gather_end(g)
        upward(g)
        if g == 0:
            for later in range(2, groups):
                gather_start(later)
            loads[2].wait()
        if g + 1 < groups:
            gather_relay(g + 1)
        if g >= 1:
            hidden_relay(g - 1)
        if g >= 2:
            downward(g - 2)
        if g >= 3:
            combine(g - 3)
    hidden_relay(groups - 1)
    for g in range(max(0, groups - 2), groups):
        downward(g)
        if g >= 1:
            combine(g - 1)

    lane = lax.broadcasted_iota(jnp.int32, (tok_rows, 128), 1)
    r_0, r_1 = routing[:, 0:1], routing[:, 1:2]
    member = jnp.zeros((tok_rows, 128), F32)
    for k in range(planes):
        named = ((r_0 == expert[k]) | (r_1 == expert[k])).astype(F32)
        member = jnp.where(lane == k, named, member)
    before = (token_col < token_row).astype(F32).astype(BF16)
    slot = dot(before, member.astype(BF16))
    slot_lane = lax.broadcasted_iota(jnp.int32, (tok_rows, cap), 1).astype(F32)
    w_0, w_1 = route_weight[:, 0:1], route_weight[:, 1:2]

    def share(k):
        weight = jnp.where(r_0 == expert[k], w_0, jnp.where(r_1 == expert[k], w_1, 0.0))
        table = jnp.where(slot_lane == slot[:, k : k + 1], weight, 0.0)
        high = table.astype(BF16)
        rest = table - high.astype(F32)
        middle = rest.astype(BF16)
        low = (rest - middle.astype(F32)).astype(BF16)
        block = comb[k]
        return dot(high, block) + (dot(middle, block) + dot(low, block))

    combine(groups - 1)
    mixed = share(0)
    for k in range(1, planes):
        back[k].wait_recv()
        mixed = mixed + share(k)

    square = jnp.sum(mixed * mixed, axis=1, keepdims=True)
    sq_out[...] = jnp.transpose(jnp.broadcast_to(square, (tok_rows, 128)))[0:8, :]
    sums = [remote(sq_out, sq_in.at[j], sq_s.at[j], sq_r.at[j], tp_peer[j]) for j in range(1, n)]
    for copy in sums:
        start(copy)
    total = sq_out[...]
    for j in range(1, n):
        sums[j - 1].wait_recv()
        total = total + sq_in[j]
    column = jnp.transpose(jnp.broadcast_to(total[0:1, :], (128, tok_rows)))[:, 0:1]
    out[...] = (mixed * lax.rsqrt(column / depth + EPS) * final_gain[...]).astype(BF16)
    for copy in sent:
        copy.wait_send()


def shards(
    tokens, norm_gain, routing, route_weight, gate_weight, up_weight, down_weight, final_gain
):
    ep_count, n = lax.axis_size("ep"), lax.axis_size("tp")
    planes = ep_count // 2
    tok_rows, width = tokens.shape
    capacity = 2 * ((tok_rows * TOPK * 5 + planes * 8 - 1) // (planes * 8))
    cap = -(-capacity // 16) * 16
    groups = min(4, planes)
    per = planes // groups
    rows = per * cap
    depth, inner = gate_weight.shape[1:]
    dma = pltpu.SemaphoreType.DMA
    vmem, anywhere = pl.BlockSpec(memory_space=pltpu.VMEM), pl.BlockSpec(memory_space=pl.ANY)
    return pl.pallas_call(
        functools.partial(kernel, n, planes, groups),
        out_shape=jax.ShapeDtypeStruct((tok_rows, width), BF16),
        in_specs=[vmem] * 5 + [anywhere] * 3 + [vmem],
        out_specs=vmem,
        scratch_shapes=[
            pltpu.VMEM((depth, inner), BF16),
            pltpu.VMEM((depth, inner), BF16),
            pltpu.VMEM((n * inner, width), BF16),
            pltpu.VMEM((n, 1, width), F32),
            pltpu.VMEM((planes, cap, width), BF16),
            pltpu.VMEM((groups, n, 2, per, cap, width), BF16),
            pltpu.VMEM((2 * rows, depth), BF16),
            pltpu.VMEM((groups, n, 2, rows, inner), BF16),
            pltpu.VMEM((groups, rows, width), BF16),
            pltpu.VMEM((groups, rows, width), BF16),
            pltpu.VMEM((groups, rows, width), BF16),
            pltpu.VMEM((groups, per, cap, width), BF16),
            pltpu.VMEM((planes, cap, width), BF16),
            pltpu.VMEM((8, 128), F32),
            pltpu.VMEM((n, 8, 128), F32),
            dma((3,)), dma((n,)), dma((n,)), dma((planes,)), dma((planes,)),
            dma((groups, n)), dma((groups, n)), dma((groups, n)), dma((groups, n)),
            dma((groups, 2, n)), dma((groups, 2, n)), dma((groups,)), dma((groups,)),
            dma((planes,)), dma((planes,)), dma((n,)), dma((n,)),
        ],
        compiler_params=pltpu.CompilerParams(
            collective_id=0, has_side_effects=True, vmem_limit_bytes=60 * 1024 * 1024
        ),
    )(
        tokens, norm_gain.reshape(1, width), routing, routing.T, route_weight,
        gate_weight, up_weight, down_weight, final_gain.reshape(1, width),
    )


def solution(mesh):
    placed = (
        P("ep", "tp"),
        P("tp"),
        P("ep", None),
        P("ep", None),
        P("ep", None, "tp"),
        P("ep", None, "tp"),
        P("ep", None, "tp"),
        P("tp"),
    )
    return jax.shard_map(
        shards, mesh=mesh, in_specs=placed, out_specs=P("ep", "tp"), check_vma=False
    )
```

time: 191 us -> 92 us (0.48)
  waiting for transfers between devices: 94.6 us -> 0 us
  Pallas kernels: 0 us -> 87.4 us
  blocking collectives: 58.8 us -> 0 us
  matrix products: 17.6 us -> 0 us
  between operations: 13.5 us -> 0.01 us
  other arithmetic: 4.71 us -> 0 us
  local copies, waits for them, and re-layouts: 1.57 us -> 4.38 us
    all_gather x2 -> x0, waiting for transfers between devices: 92.5 us -> none  [the longest x1 56 us: shards(): lax.all_gather(hidden, 'tp', axis=1, tiled=True)]
    pallas_call x0 -> x1, Pallas kernels: none -> 87.4 us  [shards(): pl.pallas_call(functools.partial(kernel, n, planes, groups), out_shape=ja...]
    all_to_all x2 -> x0, blocking collectives: 38.4 us -> none  [the longest x1 22.9 us: shards(): lax.all_to_all(outgoing, 'ep', split_axis=0, concat_axis=0, tiled=True)]
    psum x2 -> x0, blocking collectives: 20.3 us -> none  [the longest x1 11.4 us: shards(): square_sum = lax.psum(jnp.sum(values_f * values_f, axis=1), 'tp')]
    dot_general x5 -> x0, matrix products: 17.6 us -> none  [the longest x1 5.96 us: shards(): jnp.dot(lax.all_gather(hidden, 'tp', axis=1, tiled=True), down_local, pre...]
    unnamed x7 -> x3, local copies, waits for them, and re-layouts: 0.8 us -> 4.38 us
    ppermute x1 -> x0, waiting for transfers between devices: 2.07 us -> none  [from_partner(): lax.ppermute(shard, axis, [(i, i ^ 1 << apart) for i in range(lax.axis_si...]
  transfers between devices with their start and end apart: 3 -> 0, of which waited for: 3 -> 0; matrix products, arithmetic and copies ran while one was open for 0% -> 0% of each run, Pallas kernels for 0% -> 0%
where the time goes in v1:
time: 92 us; the launch traced here: 91.8 us
  Pallas kernels  87.4 us (95%)
  local copies, waits for them, and re-layouts  4.38 us (5%)
    pallas_call x1, Pallas kernels, shards(): pl.pallas_call(functools.partial(kernel, n, planes, groups), out_shape=ja...  87.4 us
    unnamed x3, local copies, waits for them, and re-layouts  4.38 us

profile of v1, /device:TPU:0, one launch (start us, length us, event | category | flops | bytes accessed | tf_op | source)
XLA Modules:
  0.0 91.8 jit_solution(1302308228729518002)
XLA Ops:
  0.0 1.4 %copy.10.route_weight = f32[128,2]{1,0:T(8,128)} copy(f32[128,2]{0,1:T(2,128)} %param.11) | data formatting | bytes 2048 | tf_op args[3]
  1.4 1.4 %copy.9.routing = s32[128,2]{1,0:T(8,128)} copy(s32[128,2]{0,1:T(2,128)} %param.10) | data formatting | bytes 2048 | tf_op args[2]
  2.8 87.4 %shard_map.82 = bf16[128,512]{1,0:T(8,128)(2,1)} custom-call(bf16[128,512]{1,0:T(8,128)(2,1)} %tokens.1, f32[1,512]{1,0:T(1,128)} %bitcast.4, s32[128,2]{1,0:T(8,128)} %copy.9.routing, s32[2,128]{1,0:T(2,128)} %bitcast.3, f32[128,2]{1,0:T(8,128)} %copy.10.route_weight, bf16[1,2048,896]{2,1,0:T(8,128)(2,1)} %gate_hbm.1, bf16[1,2048,896]{2,1,0:T(8,128)(2,1)} %up_hbm.1, ...), custom_call_target="tpu_custom_call" | custom-call | tf_op jit(solution)/shard_map/pallas_call | solution.py:327
  90.3 1.6 %copy.12 = bf16[128,512]{1,0:T(8,128)(2,1)} copy(bf16[128,512]{1,0:T(8,128)(2,1)} %shard_map.82) | data formatting | bytes 262144

commit v2 on v1

--- a/solution.py
+++ b/solution.py
@@ -26,9 +26,13 @@
     return jnp.dot(a, b, preferred_element_type=F32)
 
 
+def dot_t(a, b):
+    return lax.dot_general(a, b, (((0,), (0,)), ((), ())), preferred_element_type=F32)
+
+
 def kernel(
     n, planes, groups,
-    tokens, gain, routing, routing_t, route_weight, gate_hbm, up_hbm, down_hbm, final_gain,
+    tokens, gain, routing_t, weight_t, gate_hbm, up_hbm, down_hbm, final_gain,
     out,
     wg, wu, wd, gains, picked, x, xn, hid, half_own, half_send, half_recv, pair, comb, sq_out, sq_in,
     w_sem, gain_s, gain_r, disp_s, disp_r, x_s, x_r, d2d_s, d2d_r, h_s, h_r, po_s, po_r, c_s, c_r,
@@ -183,6 +187,8 @@
             right = dot(xn[...], wu[:, first:last])
             value = (jax.nn.silu(left) * right).astype(BF16)
             hid[g, 0, :, :, first:last] = value.reshape(2, rows, last - first)
+
+    def hidden_start(g):
         for step in range(len(bits)):
             for side in range(2):
                 copies, need, _ = hidden_trees[g][side]
@@ -202,13 +208,12 @@
     ]
 
     def downward(g):
-        for side in range(2):
-            copies, need, arrivals = hidden_trees[g][side]
-            for j in arrivals:
-                if not need[j]:
-                    copies[j].wait_recv()
         total = None
         for j in range(n):
+            for side in range(2):
+                copies, need, _ = hidden_trees[g][side]
+                if j and not need[j]:
+                    copies[j].wait_recv()
             part = wd[pl.ds(pl.multiple_of(tp_index[j] * inner, inner), inner), :]
             term = dot(hid[g, j].reshape(2 * rows, inner), part)
             total = term if total is None else total + term
@@ -233,16 +238,16 @@
             else:
                 start(back[k])
 
-    gather_start(0)
     gain_copies = [
         remote(gain, gains.at[j], gain_s.at[j], gain_r.at[j], tp_peer[j]) for j in range(1, n)
     ]
+    gather_start(0)
     for copy in gain_copies:
         start(copy)
     gains[0] = gain[...]
-    if groups > 1:
-        gather_start(1)
-    gather_relay(0)
+    for g in range(1, groups):
+        gather_start(g)
+        gather_relay(g - 1)
     for copy in gain_copies:
         copy.wait_recv()
     loads[0].wait()
@@ -251,49 +256,35 @@
         gather_end(g)
         upward(g)
         if g == 0:
-            for later in range(2, groups):
-                gather_start(later)
-            loads[2].wait()
-        if g + 1 < groups:
-            gather_relay(g + 1)
-        if g >= 1:
-            hidden_relay(g - 1)
-        if g >= 2:
-            downward(g - 2)
-        if g >= 3:
-            combine(g - 3)
-    hidden_relay(groups - 1)
-    for g in range(max(0, groups - 2), groups):
+            gather_relay(groups - 1)
+        hidden_start(g)
+    loads[2].wait()
+    turn = list(range(1, groups)) + [0]
+    for g in turn:
+        hidden_relay(g)
+    for position, g in enumerate(turn):
         downward(g)
-        if g >= 1:
-            combine(g - 1)
-
-    lane = lax.broadcasted_iota(jnp.int32, (tok_rows, 128), 1)
-    r_0, r_1 = routing[:, 0:1], routing[:, 1:2]
-    member = jnp.zeros((tok_rows, 128), F32)
-    for k in range(planes):
-        named = ((r_0 == expert[k]) | (r_1 == expert[k])).astype(F32)
-        member = jnp.where(lane == k, named, member)
-    before = (token_col < token_row).astype(F32).astype(BF16)
-    slot = dot(before, member.astype(BF16))
-    slot_lane = lax.broadcasted_iota(jnp.int32, (tok_rows, cap), 1).astype(F32)
-    w_0, w_1 = route_weight[:, 0:1], route_weight[:, 1:2]
+        if position:
+            combine(turn[position - 1])
+
+    w_t0, w_t1 = weight_t[0:1, :], weight_t[1:2, :]
 
     def share(k):
-        weight = jnp.where(r_0 == expert[k], w_0, jnp.where(r_1 == expert[k], w_1, 0.0))
-        table = jnp.where(slot_lane == slot[:, k : k + 1], weight, 0.0)
+        weight = jnp.where(r_t0 == expert[k], w_t0, w_t1)
+        table = jnp.where(slot_sub == slot_t[k : k + 1, :], weight, 0.0)
         high = table.astype(BF16)
         rest = table - high.astype(F32)
         middle = rest.astype(BF16)
         low = (rest - middle.astype(F32)).astype(BF16)
         block = comb[k]
-        return dot(high, block) + (dot(middle, block) + dot(low, block))
-
-    combine(groups - 1)
-    mixed = share(0)
-    for k in range(1, planes):
-        back[k].wait_recv()
-        mixed = mixed + share(k)
+        return dot_t(high, block) + (dot_t(middle, block) + dot_t(low, block))
+
+    combine(turn[-1])
+    mixed = None
+    for k in list(range(1, planes)) + [0]:
+        if k:
+            back[k].wait_recv()
+        mixed = share(k) if mixed is None else mixed + share(k)
 
     square = jnp.sum(mixed * mixed, axis=1, keepdims=True)
     sq_out[...] = jnp.transpose(jnp.broadcast_to(square, (tok_rows, 128)))[0:8, :]
@@ -327,7 +318,7 @@
     return pl.pallas_call(
         functools.partial(kernel, n, planes, groups),
         out_shape=jax.ShapeDtypeStruct((tok_rows, width), BF16),
-        in_specs=[vmem] * 5 + [anywhere] * 3 + [vmem],
+        in_specs=[vmem] * 4 + [anywhere] * 3 + [vmem],
         out_specs=vmem,
         scratch_shapes=[
             pltpu.VMEM((depth, inner), BF16),
@@ -354,7 +345,7 @@
             collective_id=0, has_side_effects=True, vmem_limit_bytes=60 * 1024 * 1024
         ),
     )(
-        tokens, norm_gain.reshape(1, width), routing, routing.T, route_weight,
+        tokens, norm_gain.reshape(1, width), routing.T, route_weight.T,
         gate_weight, up_weight, down_weight, final_gain.reshape(1, width),
     )
 

time: 92 us -> 72.8 us (0.79)
  Pallas kernels: 87.4 us -> 71.1 us
  local copies, waits for them, and re-layouts: 4.38 us -> 1.57 us
    pallas_call x1, Pallas kernels: 87.4 us -> 71.1 us  [shards(): pl.pallas_call(functools.partial(kernel, n, planes, groups), out_shape=ja...]
    unnamed x3 -> x1, local copies, waits for them, and re-layouts: 4.38 us -> 1.57 us
where the time goes in v2:
time: 72.8 us; the launch traced here: 72.6 us
  Pallas kernels  71.1 us (98%)
  local copies, waits for them, and re-layouts  1.57 us (2%)
    pallas_call x1, Pallas kernels, shards(): pl.pallas_call(functools.partial(kernel, n, planes, groups), out_shape=ja...  71.1 us
    unnamed x1, local copies, waits for them, and re-layouts  1.57 us

profile of v2, /device:TPU:0, one launch (start us, length us, event | category | flops | bytes accessed | tf_op | source)
XLA Modules:
  0.0 72.6 jit_solution(5671073206776392725)
XLA Ops:
  0.0 71.1 %shard_map.82 = bf16[128,512]{1,0:T(8,128)(2,1)} custom-call(bf16[128,512]{1,0:T(8,128)(2,1)} %tokens.1, f32[1,512]{1,0:T(1,128)} %bitcast.4, s32[2,128]{1,0:T(2,128)} %bitcast.6, f32[2,128]{1,0:T(2,128)} %bitcast.7, bf16[1,2048,896]{2,1,0:T(8,128)(2,1)} %gate_hbm.1, bf16[1,2048,896]{2,1,0:T(8,128)(2,1)} %up_hbm.1, bf16[1,3584,512]{2,1,0:T(8,128)(2,1)} %down_hbm.1, ...), custom_call_target="tpu_custom_call" | custom-call | tf_op jit(solution)/shard_map/pallas_call | solution.py:318
  71.1 1.6 %copy.10 = bf16[128,512]{1,0:T(8,128)(2,1)} copy(bf16[128,512]{1,0:T(8,128)(2,1)} %shard_map.82) | data formatting | bytes 262144

commit v3 on v2

--- a/solution.py
+++ b/solution.py
@@ -32,7 +32,7 @@
 
 def kernel(
     n, planes, groups,
-    tokens, gain, routing_t, weight_t, gate_hbm, up_hbm, down_hbm, final_gain,
+    tokens, gain, routing_t, weight_t, gate_hbm, up_hbm, down_hbm,
     out,
     wg, wu, wd, gains, picked, x, xn, hid, half_own, half_send, half_recv, pair, comb, sq_out, sq_in,
     w_sem, gain_s, gain_r, disp_s, disp_r, x_s, x_r, d2d_s, d2d_r, h_s, h_r, po_s, po_r, c_s, c_r,
@@ -245,9 +245,9 @@
     for copy in gain_copies:
         start(copy)
     gains[0] = gain[...]
-    for g in range(1, groups):
+    gather_relay(0)
+    for g in range(1, min(3, groups)):
         gather_start(g)
-        gather_relay(g - 1)
     for copy in gain_copies:
         copy.wait_recv()
     loads[0].wait()
@@ -256,8 +256,14 @@
         gather_end(g)
         upward(g)
         if g == 0:
-            gather_relay(groups - 1)
+            for later in range(1, groups):
+                if later >= 3:
+                    gather_start(later)
+                if later == 1:
+                    gather_relay(1)
         hidden_start(g)
+        if g + 2 < groups:
+            gather_relay(g + 2)
     loads[2].wait()
     turn = list(range(1, groups)) + [0]
     for g in turn:
@@ -296,7 +302,7 @@
         sums[j - 1].wait_recv()
         total = total + sq_in[j]
     column = jnp.transpose(jnp.broadcast_to(total[0:1, :], (128, tok_rows)))[:, 0:1]
-    out[...] = (mixed * lax.rsqrt(column / depth + EPS) * final_gain[...]).astype(BF16)
+    out[...] = mixed * lax.rsqrt(column / depth + EPS)
     for copy in sent:
         copy.wait_send()
 
@@ -315,10 +321,10 @@
     depth, inner = gate_weight.shape[1:]
     dma = pltpu.SemaphoreType.DMA
     vmem, anywhere = pl.BlockSpec(memory_space=pltpu.VMEM), pl.BlockSpec(memory_space=pl.ANY)
-    return pl.pallas_call(
+    scaled = pl.pallas_call(
         functools.partial(kernel, n, planes, groups),
-        out_shape=jax.ShapeDtypeStruct((tok_rows, width), BF16),
-        in_specs=[vmem] * 4 + [anywhere] * 3 + [vmem],
+        out_shape=jax.ShapeDtypeStruct((tok_rows, width), F32),
+        in_specs=[vmem] * 4 + [anywhere] * 3,
         out_specs=vmem,
         scratch_shapes=[
             pltpu.VMEM((depth, inner), BF16),
@@ -346,8 +352,9 @@
         ),
     )(
         tokens, norm_gain.reshape(1, width), routing.T, route_weight.T,
-        gate_weight, up_weight, down_weight, final_gain.reshape(1, width),
+        gate_weight, up_weight, down_weight,
     )
+    return (scaled * final_gain).astype(BF16)
 
 
 def solution(mesh):

time: 72.8 us -> 73.3 us (level)
  other arithmetic: 0 us -> 1.63 us
  local copies, waits for them, and re-layouts: 1.57 us -> 0.01 us
    convert_element_type x0 -> x1, other arithmetic: none -> 1.63 us  [shards(): return (scaled * final_gain).astype(BF16)]
    unnamed x1 -> x2, local copies, waits for them, and re-layouts: 1.57 us -> 0.01 us
where the time goes in v3:
time: 73.3 us; the launch traced here: 73.1 us
  Pallas kernels  71.5 us (98%)
  other arithmetic  1.63 us (2%)
    pallas_call x1, Pallas kernels, shards(): pl.pallas_call(functools.partial(kernel, n, planes, groups), out_shape=ja...  71.5 us
    convert_element_type x1, other arithmetic, shards(): return (scaled * final_gain).astype(BF16)  1.63 us

profile of v3, /device:TPU:0, one launch (start us, length us, event | category | flops | bytes accessed | tf_op | source)
XLA Modules:
  0.0 73.1 jit_solution(182599900612774529)
XLA Ops:
  0.0 0.0 copy-start
  0.0 71.5 %shard_map.82 = f32[128,512]{1,0:T(8,128)} custom-call(bf16[128,512]{1,0:T(8,128)(2,1)} %tokens.1, f32[1,512]{1,0:T(1,128)} %bitcast.3, s32[2,128]{1,0:T(2,128)} %bitcast.4, f32[2,128]{1,0:T(2,128)} %bitcast.5, bf16[1,2048,896]{2,1,0:T(8,128)(2,1)} %gate_hbm.1, bf16[1,2048,896]{2,1,0:T(8,128)(2,1)} %up_hbm.1, bf16[1,3584,512]{2,1,0:T(8,128)(2,1)} %down_hbm.1), custom_call_target="tpu_custom_call" | custom-call | tf_op jit(solution)/shard_map/pallas_call | solution.py:324
  71.5 0.0 copy-done
  71.5 1.6 %multiply_convert_fusion = bf16[128,512]{1,0:T(8,128)(2,1)} fusion(f32[128,512]{1,0:T(8,128)} %shard_map.82, f32[512]{0:T(512)S(1)} %copy-done), kind=kLoop, calls=%fused_computation | loop fusion | flops 131072 | bytes 395264 | tf_op jit(solution)/shard_map/convert_element_type | solution.py:357
Async XLA Ops:
  0.0 71.5 %copy-start = (f32[512]{0:T(512)S(1)}, f32[512]{0:T(512)}, u32[]{:S(2)}) copy-start(f32[512]{0:T(512)} %param.15) | copy-start | bytes 6148
